TPU v7x, 256 devices: a 4x2x16 block of a 4x16x16 slice. The times are simulated.
256 devices in a mesh: grp: 2 (over y), fs: 16 (over z), tp: 8 (over x, core).
Axes of the slice: x: 4, y: 2, z: 16, core: 2. Of those that a mesh axis runs over, the one named last changes fastest.
The devices are a block of a 4x16x16 slice.
Arguments:
- tokens: bfloat16 [12288, 2048], P(('grp', 'fs'), 'tp'), parts along dimension 0, may hold values from -25 to 25
- gain_first: float32 [2048], replicated, may hold values from 0.1 to 1.9
- gate_first: bfloat16 [2048, 5120], P('fs', 'tp'), may hold values from -0.125 to 0.125
- up_first: bfloat16 [2048, 5120], P('fs', 'tp'), may hold values from -0.125 to 0.125
- down_first: bfloat16 [5120, 2048], P('tp', 'fs'), may hold values from -0.078125 to 0.078125
- gain_mixer: float32 [2048], replicated, may hold values from 0.1 to 1.9
- outer_gate: bfloat16 [2048, 1024], P('fs', 'tp'), may hold values from -0.125 to 0.125
- inner_gate: bfloat16 [2048, 1024], P('fs', 'tp'), may hold values from -0.125 to 0.125
- conv_input: bfloat16 [2048, 1024], P('fs', 'tp'), may hold values from -0.125 to 0.125
- conv_taps: float32 [3, 1024], P(None, 'tp'), may hold values from -3.5 to 3.5
- mixer_out: bfloat16 [1024, 2048], P('tp', 'fs'), may hold values from -0.1875 to 0.1875
- gain_last: float32 [2048], replicated, may hold values from 0.1 to 1.9
- gate_last: bfloat16 [2048, 5120], P('fs', 'tp'), may hold values from -0.125 to 0.125
- up_last: bfloat16 [2048, 5120], P('fs', 'tp'), may hold values from -0.125 to 0.125
- down_last: bfloat16 [5120, 2048], P('tp', 'fs'), may hold values from -0.078125 to 0.078125
Outputs:
- layer_out: bfloat16 [12288, 2048], P(('grp', 'fs'), 'tp'), parts along dimension 0
There are 2 independent parts, one for each index of `grp`. A program takes and returns all parts, laid end to end along the dimension named above; an argument that names none is the same for every part. Nothing has to cross between parts.
All inputs are finite; a program needn't handle non-finite values.
Results may differ from a plain program's by a relative error of at most 0.015.
Values may be sent and summed in bfloat16 or wider, within the bound.
A program may use at most 64 MiB of HBM per device.

v0:
```python
import jax
import jax.numpy as jnp
from jax import lax
from jax.sharding import PartitionSpec as P

SEQ_LEN = 64


norm_eps = 1e-06


def turned_gather(arrays, axis, dims):
    turned = [jnp.moveaxis(a, dim, 0) for a, dim in zip(arrays, dims)]
    widths = [t[0].size for t in turned]
    both = jnp.concatenate([t.reshape(-1, w) for t, w in zip(turned, widths)], axis=1)
    whole = lax.all_gather(both, axis, axis=0, tiled=True)
    tiles = jnp.split(whole, [sum(widths[:k]) for k in range(1, len(widths))], axis=1)
    return tuple(
        (
            jnp.moveaxis(b.reshape(-1, *t.shape[1:]), 0, dim)
            for b, t, dim in zip(tiles, turned, dims)
        )
    )


def from_everyone(array, axis):
    peers = lax.axis_size(axis)
    return lax.all_to_all(
        jnp.broadcast_to(array[None], (peers, *array.shape)), axis, 0, 0, tiled=True
    )


def of_everyone(array, axis):
    everything = from_everyone(array, axis)
    return jnp.sum(everything, axis=0)


def laid_out(tiles, dim):
    tiles = jnp.moveaxis(tiles, 0, dim)
    dims = tiles.shape
    return tiles.reshape(*dims[:dim], dims[dim] * dims[dim + 1], *dims[dim + 2 :])


def collect(array, axis, dim):
    return laid_out(from_everyone(array, axis), dim)


def cut_along(array, dim, peers):
    before, after = (array.shape[:dim], array.shape[dim + 1 :])
    return jnp.moveaxis(array.reshape(*before, peers, -1, *after), dim, 0)


def summed_on_arrival(array, axis, dim):
    tiles = cut_along(array, dim, lax.axis_size(axis))
    arrived = lax.all_to_all(tiles, axis, split_axis=0, concat_axis=0, tiled=True)
    return arrived.astype(jnp.float32).sum(axis=0)


def scaled_rows(residual, gain_vec, inverse):
    return (residual * inverse * gain_vec).astype(jnp.bfloat16)


def causal_mixing(gated, conv_taps):
    row_count, channels = gated.shape
    shaped = gated.reshape(row_count // SEQ_LEN, SEQ_LEN, channels)
    kernel = conv_taps.shape[0]
    padded = jnp.pad(shaped, ((0, 0), (kernel - 1, 0), (0, 0)))
    result = jnp.zeros_like(shaped)
    for offset in range(kernel):
        result = result + conv_taps[offset] * padded[:, offset : offset + SEQ_LEN]
    return result.reshape(row_count, channels)


def shards(
    tokens,
    gain_first,
    gate_first,
    up_first,
    down_first,
    gain_mixer,
    outer_gate,
    inner_gate,
    conv_input,
    conv_taps,
    mixer_out,
    gain_last,
    gate_last,
    up_last,
    down_last,
):
    column_count = tokens.shape[1]
    tp_index = lax.axis_index("tp")
    gathered = turned_gather(
        (
            gate_first,
            up_first,
            down_first,
            outer_gate,
            inner_gate,
            conv_input,
            mixer_out,
            gate_last,
            up_last,
            down_last,
        ),
        "fs",
        (0, 0, 1, 0, 0, 0, 1, 0, 0, 1),
    )

    def channel_mixer(normed, gate_weight, up_weight, down_weight):
        gate_pre = jnp.dot(normed, gate_weight, preferred_element_type=jnp.float32)
        up_pre = jnp.dot(normed, up_weight, preferred_element_type=jnp.float32)
        hidden = (jax.nn.silu(gate_pre) * up_pre).astype(jnp.bfloat16)
        return jnp.dot(hidden, down_weight, preferred_element_type=jnp.float32)

    residual = tokens.astype(jnp.float32)

    def normalize(residual, gain_vec):
        own_gain = lax.dynamic_slice_in_dim(gain_vec, tp_index * column_count, column_count)
        squares = of_everyone(jnp.sum(residual * residual, axis=1, keepdims=True), "tp")
        inverse = lax.rsqrt(squares / gain_vec.shape[0] + norm_eps)
        return collect(scaled_rows(residual, own_gain, inverse), "tp", 1)

    def add_branch(residual, branch, factor):
        return residual + factor * summed_on_arrival(branch.astype(jnp.bfloat16), "tp", 1)

    normed = normalize(residual, gain_first)
    residual = add_branch(
        residual, channel_mixer(normed, gathered[0], gathered[1], gathered[2]), 0.5
    )
    normed = normalize(residual, gain_mixer)
    outer_pre = jnp.dot(normed, gathered[3], preferred_element_type=jnp.float32)
    inner_pre = jnp.dot(normed, gathered[4], preferred_element_type=jnp.float32)
    value_pre = jnp.dot(normed, gathered[5], preferred_element_type=jnp.float32)
    convolved = causal_mixing(inner_pre * value_pre, conv_taps)
    mixed_rows = (outer_pre * convolved).astype(jnp.bfloat16)
    residual = add_branch(
        residual, jnp.dot(mixed_rows, gathered[6], preferred_element_type=jnp.float32), 1.0
    )
    normed = normalize(residual, gain_last)
    residual = add_branch(
        residual, channel_mixer(normed, gathered[7], gathered[8], gathered[9]), 0.5
    )
    return residual.astype(jnp.bfloat16)


def solution(mesh):
    in_specs = (
        P(("grp", "fs"), "tp"),
        P(),
        P("fs", "tp"),
        P("fs", "tp"),
        P("tp", "fs"),
        P(),
        P("fs", "tp"),
        P("fs", "tp"),
        P("fs", "tp"),
        P(None, "tp"),
        P("tp", "fs"),
        P(),
        P("fs", "tp"),
        P("fs", "tp"),
        P("tp", "fs"),
    )
    out_specs = P(("grp", "fs"), "tp")
    return jax.shard_map(shards, mesh=mesh, in_specs=in_specs, out_specs=out_specs, check_vma=False)
```

profile of v0, /device:TPU:33, one launch (start us, length us, event | category | flops | bytes accessed | tf_op | source)
XLA Modules:
  0.0 424.9 jit_solution(18400280690095559362)
XLA Ops:
  6.6 0.9 copy.36
  7.5 0.9 copy.37
  8.3 0.9 copy.38
  9.2 1.1 copy.34
  10.3 1.1 copy.35
  11.4 1.1 copy.39
  12.5 1.1 copy.40
  13.9 1.0 copy-done.2
  15.7 23.7 %all-to-all-start = ((f32[8,384,1]{1,2,0:T(1,128)}), f32[8,384,1]{1,2,0:T(1,128)S(1)}, u32[]{:S(2)}, u32[]{:S(2)}) async-start(f32[8,384,1]{1,2,0:T(1,128)} %broadcast_in_dim.12), calls=%async_computation | async-start | bytes 24576 | tf_op jit(solution)/shard_map/all_to_all | solution.py:28
  39.4 0.8 dynamic_slice.9
  40.2 3.9 all-to-all-done
  44.6 23.8 %all_to_all.45 = bf16[8,384,256]{1,2,0:T(8,128)(2,1)S(1)} all-to-all(bf16[8,384,256]{1,2,0:T(8,128)(2,1)S(1)} %broadcast_in_dim.13), channel_id=1, replica_groups=mesh['grp'=2,'fs'=16,'tp'=8] {'tp'}, dimensions={0} | all-to-all | bytes 3145728 | tf_op jit(solution)/shard_map/all_to_all | solution.py:28
  68.4 166.4 %all-gather.2.cloned.1.call-done = bf16[2048,4352]{0,1:T(8,128)(2,1)} async-done(((bf16[128,4352]{0,1:T(8,128)(2,1)}), bf16[2048,4352]{0,1:T(8,128)(2,1)}) %all-gather.2.cloned.1.call-update) | async-done | bytes 17825808 | tf_op jit(solution)/shard_map/all_gather | solution.py:16
  234.8 4.2 fusion.8
  238.9 5.9 %convolution_convert_fusion.1 = bf16[384,2048]{1,0:T(8,128)(2,1)S(1)} fusion(bf16[2048,4352]{0,1:T(8,128)(2,1)} %all-gather.2.cloned.1.call-done, bf16[384,2048]{0,1:T(8,128)(2,1)S(1)} %bitcast.59, f32[384,640]{1,0:T(8,128)} %fusion.8), kind=kOutput, calls=%fused_computation.4 | convolution fusion | flops 2015526912 | bytes 9371648 | tf_op jit(solution)/shard_map/dot_general | solution.py:114
  244.9 34.9 %all_to_all.46 = bf16[8,384,256]{2,1,0:T(8,128)(2,1)S(1)} all-to-all(bf16[8,384,256]{2,1,0:T(8,128)(2,1)S(1)} %bitcast.55), channel_id=1, replica_groups=mesh['grp'=2,'fs'=16,'tp'=8] {'tp'}, dimensions={0} | all-to-all | bytes 3145728 | tf_op jit(solution)/shard_map/all_to_all | solution.py:55
  280.8 4.3 %all-to-all-start.3 = ((f32[8,384,1]{1,2,0:T(1,128)}), f32[8,384,1]{1,2,0:T(1,128)S(1)}, u32[]{:S(2)}, u32[]{:S(2)}) async-start(f32[8,384,1]{1,2,0:T(1,128)} %broadcast_in_dim.14), calls=%async_computation.3 | async-start | bytes 24576 | tf_op jit(solution)/shard_map/all_to_all | solution.py:28
  285.9 3.9 all-to-all-done.3
  290.2 1.3 broadcast_in_dim.15
  291.5 4.3 %all-to-all-start.4 = ((bf16[8,384,256]{1,2,0:T(8,128)(2,1)}), bf16[8,384,256]{1,2,0:T(8,128)(2,1)S(1)}, u32[]{:S(2)}, u32[]{:S(2)}) async-start(bf16[8,384,256]{1,2,0:T(8,128)(2,1)} %broadcast_in_dim.15), calls=%async_computation.4 | async-start | bytes 3145728 | tf_op jit(solution)/shard_map/all_to_all | solution.py:28
  295.8 20.7 %all-to-all-done.4 = bf16[8,384,256]{1,2,0:T(8,128)(2,1)S(1)} async-done(((bf16[8,384,256]{1,2,0:T(8,128)(2,1)}), bf16[8,384,256]{1,2,0:T(8,128)(2,1)S(1)}, u32[]{:S(2)}, u32[]{:S(2)}) %all-to-all-start.4) | async-done | bytes 1572896 | tf_op jit(solution)/shard_map/all_to_all | solution.py:28
  316.5 1.6 fusion.35
  318.2 1.6 convolution_multiply_fusion
  320.5 3.1 convolution_convert_fusion.2
  323.8 24.0 %all_to_all.47 = bf16[8,384,256]{2,1,0:T(8,128)(2,1)S(1)} all-to-all(bf16[8,384,256]{2,1,0:T(8,128)(2,1)S(1)} %bitcast.56), channel_id=1, replica_groups=mesh['grp'=2,'fs'=16,'tp'=8] {'tp'}, dimensions={0} | all-to-all | bytes 3145728 | tf_op jit(solution)/shard_map/all_to_all | solution.py:55
  349.5 4.3 %all-to-all-start.6 = ((f32[8,384,1]{1,2,0:T(1,128)}), f32[8,384,1]{1,2,0:T(1,128)S(1)}, u32[]{:S(2)}, u32[]{:S(2)}) async-start(f32[8,384,1]{1,2,0:T(1,128)} %broadcast_in_dim.16), calls=%async_computation.6 | async-start | bytes 24576 | tf_op jit(solution)/shard_map/all_to_all | solution.py:28
  353.8 0.8 dynamic_slice.11
  354.6 3.9 all-to-all-done.6
  359.0 23.8 %all_to_all.48 = bf16[8,384,256]{1,2,0:T(8,128)(2,1)S(1)} all-to-all(bf16[8,384,256]{1,2,0:T(8,128)(2,1)S(1)} %broadcast_in_dim.17), channel_id=1, replica_groups=mesh['grp'=2,'fs'=16,'tp'=8] {'tp'}, dimensions={0} | all-to-all | bytes 3145728 | tf_op jit(solution)/shard_map/all_to_all | solution.py:28
  382.8 4.2 fusion.3
  386.9 5.9 %convolution_convert_fusion = bf16[384,2048]{1,0:T(8,128)(2,1)S(1)} fusion(bf16[2048,4352]{0,1:T(8,128)(2,1)} %all-gather.2.cloned.1.call-done, bf16[384,2048]{0,1:T(8,128)(2,1)S(1)} %bitcast.61, f32[384,640]{1,0:T(8,128)} %fusion.3), kind=kOutput, calls=%fused_computation.3 | convolution fusion | flops 2015526912 | bytes 9371648 | tf_op jit(solution)/shard_map/dot_general | solution.py:114
  392.9 24.1 %all_to_all.49 = bf16[8,384,256]{2,1,0:T(8,128)(2,1)S(1)} all-to-all(bf16[8,384,256]{2,1,0:T(8,128)(2,1)S(1)} %bitcast.57), channel_id=1, replica_groups=mesh['grp'=2,'fs'=16,'tp'=8] {'tp'}, dimensions={0} | all-to-all | bytes 3145728 | tf_op jit(solution)/shard_map/all_to_all | solution.py:55
  (55 shorter events, 7.7 us)
Async XLA Ops:
  6.5 7.1 %copy-start.3 = (bf16[640,128]{1,0:T(8,128)(2,1)S(1)}, bf16[640,128]{1,0:T(8,128)(2,1)}, u32[]{:S(2)}) copy-start(bf16[640,128]{1,0:T(8,128)(2,1)} %param.19) | copy-start | bytes 491524
  6.5 7.2 %copy-start.5 = (bf16[128,128]{1,0:T(8,128)(2,1)S(1)}, bf16[128,128]{1,0:T(8,128)(2,1)}, u32[]{:S(2)}) copy-start(bf16[128,128]{1,0:T(8,128)(2,1)} %param.25) | copy-start | bytes 98308
  6.6 228.2 %all-gather.2.cloned.1.call-start = ((), (), s32[]{:S(2)}) async-start(), calls=%async_computation.9 | async-start | bytes 18939904 | tf_op jit(solution)/shard_map/all_gather | solution.py:16
  9.2 4.6 %copy-start.4 = (bf16[640,128]{1,0:T(8,128)(2,1)S(1)}, bf16[640,128]{1,0:T(8,128)(2,1)}, u32[]{:S(2)}) copy-start(bf16[640,128]{1,0:T(8,128)(2,1)} %param.29) | copy-start | bytes 491524
  13.6 1.4 copy-start
  13.9 1.0 copy-start.2
  15.7 28.4 %all-to-all-start = ((f32[8,384,1]{1,2,0:T(1,128)}), f32[8,384,1]{1,2,0:T(1,128)S(1)}, u32[]{:S(2)}, u32[]{:S(2)}) async-start(f32[8,384,1]{1,2,0:T(1,128)} %broadcast_in_dim.12), calls=%async_computation | async-start | bytes 24576 | tf_op jit(solution)/shard_map/all_to_all | solution.py:28
  280.8 9.0 %all-to-all-start.3 = ((f32[8,384,1]{1,2,0:T(1,128)}), f32[8,384,1]{1,2,0:T(1,128)S(1)}, u32[]{:S(2)}, u32[]{:S(2)}) async-start(f32[8,384,1]{1,2,0:T(1,128)} %broadcast_in_dim.14), calls=%async_computation.3 | async-start | bytes 24576 | tf_op jit(solution)/shard_map/all_to_all | solution.py:28
  291.5 4.3 %copy-start.6 = (f32[3,128]{1,0:T(4,128)S(1)}, f32[3,128]{1,0:T(4,128)}, u32[]{:S(2)}) copy-start(f32[3,128]{1,0:T(4,128)} %param.24) | copy-start | bytes 4612
  291.5 25.0 %all-to-all-start.4 = ((bf16[8,384,256]{1,2,0:T(8,128)(2,1)}), bf16[8,384,256]{1,2,0:T(8,128)(2,1)S(1)}, u32[]{:S(2)}, u32[]{:S(2)}) async-start(bf16[8,384,256]{1,2,0:T(8,128)(2,1)} %broadcast_in_dim.15), calls=%async_computation.4 | async-start | bytes 3145728 | tf_op jit(solution)/shard_map/all_to_all | solution.py:28
  347.8 0.9 copy-start.1
  349.5 9.0 %all-to-all-start.6 = ((f32[8,384,1]{1,2,0:T(1,128)}), f32[8,384,1]{1,2,0:T(1,128)S(1)}, u32[]{:S(2)}, u32[]{:S(2)}) async-start(f32[8,384,1]{1,2,0:T(1,128)} %broadcast_in_dim.16), calls=%async_computation.6 | async-start | bytes 24576 | tf_op jit(solution)/shard_map/all_to_all | solution.py:28
Sparse Core Ops, SparseCore 0:
  15.1 219.6 all-gather.1
where the time goes:
time: 426 us; the launch traced here: 425 us
  waiting for transfers between devices  199 us (47%)
  blocking collectives  131 us (31%)
  starting transfers between devices  36.6 us (9%)
  matrix products  26.5 us (6%)
  local copies, waits for them, and re-layouts  15.5 us (4%)
  between operations  13.7 us (3%)
    all_gather x1, waiting for transfers between devices, turned_gather(): whole = lax.all_gather(both, axis, axis=0, tiled=True)  166 us
    all_to_all x3, blocking collectives, summed_on_arrival(): lax.all_to_all(tiles, axis, split_axis=0, concat_axis=0, tiled=True)  83 us
    all_to_all x2, blocking collectives, from_everyone(): lax.all_to_all(jnp.broadcast_to(array[None], (peers, *array.shape)), axis...  47.6 us
    all_to_all x4, starting transfers between devices, from_everyone(): lax.all_to_all(jnp.broadcast_to(array[None], (peers, *array.shape)), axis...  36.6 us
    all_to_all x4, waiting for transfers between devices, from_everyone(): lax.all_to_all(jnp.broadcast_to(array[None], (peers, *array.shape)), axis...  32.5 us
    dot_general x2, matrix products, channel_mixer(): return jnp.dot(hidden, down_weight, preferred_element_type=jnp.float32)  11.8 us
    unnamed x30, local copies, waits for them, and re-layouts  8.91 us
  transfers between devices with their start and end apart: 5, of which 5 were waited for; matrix products, arithmetic and copies ran while one was open for 1% of the time, Pallas kernels for 0%

commit v1 on v0

v1 whole, which is shorter than its diff:
```python
import functools

import jax
import jax.numpy as jnp
from jax import lax
from jax.experimental import pallas as pl
from jax.experimental.pallas import tpu as pltpu
from jax.sharding import PartitionSpec as P

SEQ_LEN = 64
EPS = 1e-06
MESH = pl.DeviceIdType.MESH
BF16 = jnp.bfloat16
F32 = jnp.float32

STREAMS = (("g1", 0), ("u1", 0), ("d1", 2), ("mx", 7), ("g2", 9), ("u2", 9), ("d2", 12))
PLAN = {
    ("g1", 0): ("ag_start0",),
    ("g1", 2): ("ag_pass0",),
    ("g1", 4): ("ag_far0",),
    ("g1", 6): ("norm0",),
    ("mx", 1): ("hidden1a",),
    ("d1", 7): ("hidden1b",),
    ("d1", 8): ("branch0",),
    ("g2", 2): ("pair0",),
    ("g2", 3): ("merge0",),
    ("mx", 6): ("finish0",),
    ("g2", 4): ("ag_start1",),
    ("u2", 4): ("ag_pass1",),
    ("g2", 5): ("ag_far1",),
    ("u2", 5): ("norm1",),
    ("d2", 3): ("mixer", "branch1"),
    ("u2", 7): ("pair1",),
    ("d2", 4): ("merge1",),
    ("g2", 8): ("finish1",),
    ("u2", 8): ("ag_start2",),
    ("d2", 5): ("ag_pass2",),
    ("d2", 6): ("ag_far2",),
    ("d2", 7): ("norm2",),
    ("d2", 8): ("hidden2a", "hidden2b", "branch2", "pair2", "merge2", "finish2"),
}


def own_part(rows, share, unit=16):
    return int(rows * share) // unit * unit


def layer(sizes, *refs):
    n_fs, n_tp, paired, splits = sizes
    (tokens, gain_first, gate_first, up_first, down_first, gain_mixer, outer_gate, inner_gate, conv_input, conv_taps,
     mixer_out, gain_last, gate_last, up_last, down_last, out,
     g1, u1, d1, mx, g2, u2, d2, raw, normed, hidden, mixed, res, acc, pair_out, pair_in, side_out, side_in,
     local_sem, z_send, z_recv, y_send, y_recv, x_send, x_recv) = refs
    rows, cols = tokens.shape
    half_rows = rows // 2
    half = n_fs // 2
    f = lax.axis_index("fs")
    t = lax.axis_index("tp")
    g = lax.axis_index("grp")
    n_x = n_tp // 2
    x, core = t // 2, t % 2
    par = g % 2
    depth = mx.shape[1] // 4

    up_fs, dn_fs = lax.rem(f + 1, n_fs), lax.rem(f + n_fs - 1, n_fs)
    ahead = lax.rem(x + 1, n_x) * 2 + core
    behind = lax.rem(x + n_x - 1, n_x) * 2 + core
    across = lax.rem(x + 2, n_x) * 2 + core
    partner = x * 2 + (1 - core)
    mate = g + 1 - 2 * par

    bufs = {"g1": g1, "u1": u1, "d1": d1, "mx": mx, "g2": g2, "u2": u2, "d2": d2}
    names = tuple(bufs)
    sources = {
        "g1": (gate_first,), "u1": (up_first,), "d1": (down_first,),
        "mx": (outer_gate, inner_gate, conv_input, mixer_out),
        "g2": (gate_last,), "u2": (up_last,), "d2": (down_last,),
    }

    loads = {}
    spare = 0
    own_tokens = pltpu.make_async_copy(tokens, raw.at[0, t], local_sem.at[spare])
    own_tokens.start()
    for name in names:
        loads[name] = []
        many = len(sources[name])
        for piece, source in enumerate(sources[name]):
            spare += 1
            place = bufs[name].at[f] if many == 1 else bufs[name].at[f, pl.ds(piece * depth, depth)]
            copy = pltpu.make_async_copy(source, place, local_sem.at[spare])
            copy.start()
            loads[name].append(copy)

    barrier = pltpu.get_barrier_semaphore()
    peers = [{"fs": up_fs}, {"fs": dn_fs}, {"tp": ahead}, {"tp": behind}, {"tp": partner}]
    if paired:
        peers.append({"grp": mate})
    for peer in peers:
        pl.semaphore_signal(barrier, inc=1, device_id=peer, device_id_type=MESH)
    pl.semaphore_wait(barrier, len(peers))

    def remote(source, target, send, recv, peer):
        return pltpu.make_async_remote_copy(
            src_ref=source, dst_ref=target, send_sem=send, recv_sem=recv, device_id=peer, device_id_type=MESH
        )

    in_flight = {}

    def send_slot(kind, count):
        queue = in_flight.setdefault(kind, [])
        if len(queue) == count:
            queue.pop(0).wait_send()
        position = in_flight.get((kind, "next"), 0)
        in_flight[(kind, "next")] = (position + 1) % count
        return position

    def ring_rows(name, direction, hop):
        alone, both = splits[name]
        length = alone + both
        start = par * alone
        if hop == half:
            first = (length // 2 + 15) // 16 * 16
            start, length = (start, first) if direction == 0 else (start + first, length - first)
        return pl.ds(pl.multiple_of(start, 16), length)

    def ring_copy(name, direction, hop, send=None):
        block = lax.rem(f + n_fs - (hop - 1), n_fs) if direction == 0 else lax.rem(f + hop - 1, n_fs)
        place = bufs[name].at[block, ring_rows(name, direction, hop)]
        send = 0 if send is None else send
        return remote(
            place, place, z_send.at[direction, send], z_recv.at[names.index(name), direction, hop - 1],
            {"fs": up_fs if direction == 0 else dn_fs},
        )

    def ring_start(name, direction, hop):
        slot = send_slot(("z", direction), z_send.shape[1])
        copy = ring_copy(name, direction, hop, slot)
        copy.start()
        in_flight[("z", direction)].append(copy)

    def hand_over(name, block):
        alone, both = splits[name]
        place = bufs[name].at[block, pl.ds(pl.multiple_of(par * (alone + both), 16), alone)]
        slot = send_slot("y", y_send.shape[0])
        copy = remote(place, place, y_send.at[slot], y_recv.at[names.index(name)], {"grp": mate})
        copy.start()
        in_flight["y"].append(copy)

    def ring_event(name, hop):
        if hop == 0:
            for copy in loads[name]:
                copy.wait()
            for direction in (0, 1):
                ring_start(name, direction, 1)
            return
        for direction in (0, 1):
            ring_copy(name, direction, hop).wait_recv()
            if hop < half:
                ring_start(name, direction, hop + 1)
        if paired:
            hand_over(name, lax.rem(f + n_fs - hop, n_fs))
            if hop < half:
                hand_over(name, lax.rem(f + hop, n_fs))

    def whole(name):
        if paired:
            alone = splits[name][0]
            view = bufs[name].at[pl.ds(0, n_fs - 1), pl.ds(0, alone)]
            pltpu.make_async_copy(view, view, y_recv.at[names.index(name)]).wait()

    x_flight = {}

    def x_start(number, phase, source, target, peer):
        if number in x_flight:
            x_flight[number].wait_send()
        copy = remote(source, target, x_send.at[number], x_recv.at[phase, number], peer)
        copy.start()
        x_flight[number] = copy

    def x_wait(number, phase, place):
        remote(place, place, x_send.at[number], x_recv.at[phase, number], {"tp": ahead}).wait_recv()

    low, high = pl.ds(0, half_rows), pl.ds(half_rows, half_rows)

    def ag_start(phase):
        if phase == 0:
            own_tokens.wait()
        own = raw.at[phase, t]
        x_start(0, phase, own, own, {"tp": ahead})
        x_start(1, phase, own, own, {"tp": behind})
        x_start(2, phase, own, own, {"tp": partner})

    def ag_pass(phase):
        prev, nxt = raw.at[phase, behind], raw.at[phase, ahead]
        x_wait(0, phase, prev)
        x_start(3, phase, raw.at[phase, behind, low], raw.at[phase, behind, low], {"tp": ahead})
        x_wait(1, phase, nxt)
        x_start(4, phase, raw.at[phase, ahead, high], raw.at[phase, ahead, high], {"tp": behind})
        x_start(5, phase, prev, prev, {"tp": partner})
        x_start(6, phase, nxt, nxt, {"tp": partner})

    def ag_far(phase):
        x_wait(3, phase, raw.at[phase, across, low])
        x_wait(4, phase, raw.at[phase, across, high])
        far = raw.at[phase, across]
        x_start(7, phase, far, far, {"tp": partner})

    def norm(phase, gain):
        for number in (2, 5, 6, 7):
            x_wait(number, phase, raw.at[phase, partner])
        step = 32

        def some(i, _):
            at = pl.ds(pl.multiple_of(i * step, step), step)
            parts = [raw[phase, j, at, :].astype(F32) for j in range(n_tp)]
            total = parts[0] * parts[0]
            for part in parts[1:]:
                total = total + part * part
            inverse = lax.rsqrt(jnp.sum(total, axis=1, keepdims=True) / (n_tp * cols) + EPS)
            for j, part in enumerate(parts):
                span = pl.ds(j * cols, cols)
                normed[at, span] = (part * inverse * gain[:, span]).astype(BF16)
            return 0

        lax.fori_loop(0, rows // step, some, 0)

    def hidden_tiles(gate, up, first, last):
        width = 128

        def tile(i, _):
            span = pl.ds(pl.multiple_of(i * width, width), width)
            k = gate.shape[0] * gate.shape[1]
            both = jnp.concatenate(
                [gate[:, :, span].reshape(k, width), up[:, :, span].reshape(k, width)], axis=1
            )
            pre = jnp.dot(normed[...], both, preferred_element_type=F32)
            gate_pre, up_pre = pre[:, :width], pre[:, width:]
            hidden[:, span] = (gate_pre / (1.0 + jnp.exp(-gate_pre)) * up_pre).astype(BF16)
            return 0

        lax.fori_loop(first, last, tile, 0)

    def mixer():
        whole("mx")
        k = n_fs * depth
        weight = lambda p: mx[:, p * depth:(p + 1) * depth, :].reshape(k, mx.shape[2])
        width = mx.shape[2]
        pair = jnp.dot(normed[...], jnp.concatenate([weight(1), weight(2)], axis=1), preferred_element_type=F32)
        gated = pair[:, :width] * pair[:, width:]
        place = lax.rem(lax.broadcasted_iota(jnp.int32, gated.shape, 0), SEQ_LEN)
        kernel = conv_taps.shape[0]
        convolved = gated * conv_taps[kernel - 1:kernel, :]
        for back in range(1, kernel):
            earlier = jnp.where(place >= back, pltpu.roll(gated, back, 0), 0.0)
            convolved = convolved + earlier * conv_taps[kernel - 1 - back:kernel - back, :]
        outer = jnp.dot(normed[...], weight(0), preferred_element_type=F32)
        mixed[...] = (outer * convolved).astype(BF16)

    def block_of(left, down, lead, owner):
        per = cols // down.shape[2]
        tiles = [down[owner * per + p][lead:, :] if lead else down[owner * per + p] for p in range(per)]
        return jnp.dot(left[...], jnp.concatenate(tiles, axis=1), preferred_element_type=F32)

    def branch(phase, left, name, lead):
        whole(name) if phase != 1 else None
        down = bufs[name]
        for j in range(n_x):
            if 8 + j in x_flight:
                x_flight.pop(8 + j).wait_send()

        def theirs(j, _):
            pair_out[j] = block_of(left, down, lead, lax.rem(x + j, n_x) * 2 + 1 - core).astype(BF16)
            return 0

        lax.fori_loop(0, n_x, theirs, 0)

        def pair_copy(j):
            return remote(pair_out.at[j], pair_in.at[phase, j], x_send.at[8 + j], x_recv.at[phase, 8 + j], {"tp": partner})

        def ours(j, _):
            pair_copy(j).start()
            acc[j] = block_of(left, down, lead, lax.rem(x + j, n_x) * 2 + core)
            return 0

        lax.fori_loop(0, n_x, ours, 0)
        for j in range(n_x):
            x_flight[8 + j] = pair_copy(j)

    def pair(phase):
        for j in (2, 1, 3, 0):
            x_wait(8 + j, phase, pair_in.at[phase, j])
        for number in range(12, 18):
            if number in x_flight:
                x_flight.pop(number).wait_send()
        for direction, keep in ((0, low), (1, high)):
            side_out[direction, 0] = (acc[2, keep, :] + pair_in[phase, 2, keep, :].astype(F32)).astype(BF16)
        for direction, near, keep in ((0, 1, high), (1, 3, low)):
            side_out[direction, 1] = (acc[near, keep, :] + pair_in[phase, near, keep, :].astype(F32)).astype(BF16)
        for near, keep in ((1, low), (3, high)):
            acc[near, keep, :] = acc[near, keep, :] + pair_in[phase, near, keep, :].astype(F32)
        acc[0] = acc[0] + pair_in[phase, 0].astype(F32)
        for order in (0, 1):
            for direction in (0, 1):
                side_start(phase, direction, order)

    def side_start(phase, direction, order):
        x_start(
            12 + 2 * order + direction, phase, side_out.at[direction, order], side_in.at[phase, direction, order],
            {"tp": ahead if direction == 0 else behind},
        )

    def side_wait(phase, direction, order):
        x_wait(12 + 2 * order + direction, phase, side_in.at[phase, direction, order])

    def merge(phase, factor):
        for direction, near, keep in ((0, 1, low), (1, 3, high)):
            side_wait(phase, direction, 0)
            side_out[direction, 2] = (acc[near, keep, :] + side_in[phase, direction, 0].astype(F32)).astype(BF16)
        res[...] = res[...] + factor * acc[0]
        for direction in (0, 1):
            side_start(phase, direction, 2)

    def finish(phase, factor):
        for order in (1, 2):
            for direction in (0, 1):
                side_wait(phase, direction, order)
        lo = side_in[phase, 0, 2].astype(F32) + side_in[phase, 1, 1].astype(F32)
        hi = side_in[phase, 0, 1].astype(F32) + side_in[phase, 1, 2].astype(F32)
        last = phase == 2
        for keep, extra in ((low, lo), (high, hi)):
            value = res[keep, :] + factor * extra
            if last:
                out[keep, :] = value.astype(BF16)
            else:
                res[keep, :] = value
                raw[phase + 1, t, keep, :] = value.astype(BF16)

    def hidden1a():
        whole("g1")
        whole("u1")
        hidden_tiles(g1, u1, 0, 3)

    def hidden2a():
        whole("g2")
        whole("u2")
        hidden_tiles(g2, u2, 0, 3)

    def norm0():
        norm(0, gain_first)
        res[...] = raw[0, t].astype(F32)

    tiles = g1.shape[2] // 128
    stages = {
        "ag_start0": lambda: ag_start(0), "ag_pass0": lambda: ag_pass(0), "ag_far0": lambda: ag_far(0),
        "norm0": norm0, "hidden1a": hidden1a, "hidden1b": lambda: hidden_tiles(g1, u1, 3, tiles),
        "branch0": lambda: branch(0, hidden, "d1", 0), "pair0": lambda: pair(0), "merge0": lambda: merge(0, 0.5),
        "finish0": lambda: finish(0, 0.5),
        "ag_start1": lambda: ag_start(1), "ag_pass1": lambda: ag_pass(1), "ag_far1": lambda: ag_far(1),
        "norm1": lambda: norm(1, gain_mixer), "mixer": mixer,
        "branch1": lambda: branch(1, mixed, "mx", 3 * depth), "pair1": lambda: pair(1), "merge1": lambda: merge(1, 1.0),
        "finish1": lambda: finish(1, 1.0),
        "ag_start2": lambda: ag_start(2), "ag_pass2": lambda: ag_pass(2), "ag_far2": lambda: ag_far(2),
        "norm2": lambda: norm(2, gain_last), "hidden2a": hidden2a, "hidden2b": lambda: hidden_tiles(g2, u2, 3, tiles),
        "branch2": lambda: branch(2, hidden, "d2", 0), "pair2": lambda: pair(2), "merge2": lambda: merge(2, 0.5),
        "finish2": lambda: finish(2, 0.5),
    }

    plan = plan_for(half)
    for event in ring_order(half):
        ring_event(*event)
        for stage in plan.get(event, ()):
            stages[stage]()

    for copy in list(x_flight.values()):
        copy.wait_send()
    for key, queue in in_flight.items():
        if isinstance(queue, list):
            for copy in queue:
                copy.wait_send()


def ring_order(half):
    events = []
    for step in range(max(first for _, first in STREAMS) + half + 1):
        for name, first in STREAMS:
            if 0 <= step - first <= half:
                events.append((name, step - first))
    return events


def plan_for(half):
    if half == 8:
        return PLAN
    last = ring_order(half)[-1]
    return {last: tuple(stage for stages in PLAN.values() for stage in stages)}


def fused_layer(n_fs, n_tp, n_grp, *args):
    tokens, gate, down, outer = args[0], args[2], args[4], args[6]
    rows, cols = tokens.shape
    paired = n_grp % 2 == 0
    n_x = n_tp // 2
    depth, hid = gate.shape
    chan = outer.shape[1]

    def split(length, share):
        alone = own_part(length, share) if paired else 0
        return alone, length - 2 * alone

    splits = {
        "g1": split(depth, 0.38), "u1": split(depth, 0.3), "d1": split(hid, 0.35), "mx": split(4 * depth, 0.35),
        "g2": split(depth, 0.38), "u2": split(depth, 0.3), "d2": split(hid, 0.35),
    }
    half = n_fs // 2
    wide = pltpu.VMEM((n_fs, depth, hid), BF16)
    tall = pltpu.VMEM((n_fs, hid, depth), BF16)
    gains = {1, 5, 11}
    args = [a.reshape(1, -1) if i in gains else a for i, a in enumerate(args)]
    vmem, anywhere = pl.BlockSpec(memory_space=pltpu.VMEM), pl.BlockSpec(memory_space=pl.ANY)
    in_vmem = gains | {9}
    return pl.pallas_call(
        functools.partial(layer, (n_fs, n_tp, paired, splits)),
        out_shape=jax.ShapeDtypeStruct((rows, cols), BF16),
        in_specs=[vmem if i in in_vmem else anywhere for i in range(len(args))],
        out_specs=vmem,
        scratch_shapes=[
            wide, wide, tall, pltpu.VMEM((n_fs, 4 * depth, chan), BF16), wide, wide, tall,
            pltpu.VMEM((3, n_tp, rows, cols), BF16),
            pltpu.VMEM((rows, n_tp * cols), BF16),
            pltpu.VMEM((rows, hid), BF16),
            pltpu.VMEM((rows, chan), BF16),
            pltpu.VMEM((rows, cols), F32),
            pltpu.VMEM((n_x, rows, cols), F32),
            pltpu.VMEM((n_x, rows, cols), BF16),
            pltpu.VMEM((3, n_x, rows, cols), BF16),
            pltpu.VMEM((2, 3, rows // 2, cols), BF16),
            pltpu.VMEM((3, 2, 3, rows // 2, cols), BF16),
            pltpu.SemaphoreType.DMA((11,)),
            pltpu.SemaphoreType.DMA((2, 8)),
            pltpu.SemaphoreType.DMA((7, 2, half)),
            pltpu.SemaphoreType.DMA((8,)),
            pltpu.SemaphoreType.DMA((7,)),
            pltpu.SemaphoreType.DMA((18,)),
            pltpu.SemaphoreType.DMA((3, 18)),
        ],
        compiler_params=pltpu.CompilerParams(
            collective_id=0, has_side_effects=True, vmem_limit_bytes=60 * 1024 * 1024
        ),
        name="fused_layer",
    )(*args)


def solution(mesh):
    in_specs = (
        P(("grp", "fs"), "tp"),
        P(),
        P("fs", "tp"),
        P("fs", "tp"),
        P("tp", "fs"),
        P(),
        P("fs", "tp"),
        P("fs", "tp"),
        P("fs", "tp"),
        P(None, "tp"),
        P("tp", "fs"),
        P(),
        P("fs", "tp"),
        P("fs", "tp"),
        P("tp", "fs"),
    )
    out_specs = P(("grp", "fs"), "tp")
    body = functools.partial(fused_layer, mesh.shape["fs"], mesh.shape["tp"], mesh.shape["grp"])
    return jax.shard_map(body, mesh=mesh, in_specs=in_specs, out_specs=out_specs, check_vma=False)
```

time: 426 us -> 184 us (0.43)
  waiting for transfers between devices: 199 us -> 0 us
  Pallas kernels: 0 us -> 182 us
  blocking collectives: 131 us -> 0 us
  starting transfers between devices: 36.6 us -> 0 us
  matrix products: 26.5 us -> 0 us
  local copies, waits for them, and re-layouts: 15.5 us -> 1.62 us
  between operations: 13.7 us -> 0.01 us
    pallas_call x0 -> x1, Pallas kernels: none -> 182 us  [fused_layer(): pl.pallas_call(functools.partial(layer, (n_fs, n_tp, paired, splits)), ou...]
    all_gather x1 -> x0, waiting for transfers between devices: 166 us -> none  [turned_gather(): whole = lax.all_gather(both, axis, axis=0, tiled=True)]
    all_to_all x5 -> x0, blocking collectives: 131 us -> none  [the longest x3 83 us: summed_on_arrival(): lax.all_to_all(tiles, axis, split_axis=0, concat_axis=0, tiled=True)]
    all_to_all x4 -> x0, starting transfers between devices: 36.6 us -> none  [from_everyone(): lax.all_to_all(jnp.broadcast_to(array[None], (peers, *array.shape)), axis...]
    all_to_all x4 -> x0, waiting for transfers between devices: 32.5 us -> none  [from_everyone(): lax.all_to_all(jnp.broadcast_to(array[None], (peers, *array.shape)), axis...]
    dot_general x7 -> x0, matrix products: 26.5 us -> none  [the longest x2 11.8 us: channel_mixer(): return jnp.dot(hidden, down_weight, preferred_element_type=jnp.float32)]
    unnamed x30 -> x1, local copies, waits for them, and re-layouts: 8.91 us -> 1.62 us
  transfers between devices with their start and end apart: 5 -> 0, of which waited for: 5 -> 0; matrix products, arithmetic and copies ran while one was open for 1% -> 0% of each run, Pallas kernels for 0% -> 0%
where the time goes in v1:
time: 184 us
  Pallas kernels  182 us (99%)
    pallas_call x1, Pallas kernels, fused_layer(): pl.pallas_call(functools.partial(layer, (n_fs, n_tp, paired, splits)), ou...  182 us

profile of v1, /device:TPU:33, one launch (start us, length us, event | category | flops | bytes accessed | tf_op | source)
XLA Modules:
  0.0 183.6 jit_solution(2229620250161124821)
XLA Ops:
  0.0 182.0 %fused_layer.1 = bf16[384,256]{1,0:T(8,128)(2,1)} custom-call(bf16[384,256]{1,0:T(8,128)(2,1)} %refs_0_.1, f32[1,2048]{1,0:T(1,128)} %bitcast.3, bf16[128,640]{1,0:T(8,128)(2,1)} %refs_2_.1, bf16[128,640]{1,0:T(8,128)(2,1)} %refs_3_.1, bf16[640,128]{1,0:T(8,128)(2,1)} %refs_4_.1, f32[1,2048]{1,0:T(1,128)} %bitcast.4, bf16[128,128]{1,0:T(8,128)(2,1)} %refs_6_.1, ...), custom_call_target="tpu_custom_call" | custom-call | tf_op jit(solution)/shard_map/fused_layer/pallas_call | solution.py:421
  182.0 1.6 copy.17

commit v2 on v1

v2 whole, which is shorter than its diff:
```python
import functools

import jax
import jax.numpy as jnp
from jax import lax
from jax.experimental import pallas as pl
from jax.experimental.pallas import tpu as pltpu
from jax.sharding import PartitionSpec as P

SEQ_LEN = 64
EPS = 1e-06
MESH = pl.DeviceIdType.MESH
BF16 = jnp.bfloat16
F32 = jnp.float32

EARLY = (
    (("u1", 0), 0, ("ag_start0",)),
    (("u1", 1), 0, ("ag_pass0", "ag_mid0")),
    (("u1", 2), 0, ("ag_far0",)),
    (("u1", 3), 0, ("norm0", "hidden1a")),
    (("u1", 4), 1, ("hidden1b",)),
    (("u1", 6), 1, ("hidden1c",)),
)
LATE = (
    (2, "hidden1d"), (3, "branch0"), (6, "merge0"), (8, "finish0"),
    (10, "ag_pass1"), (11, "ag_mid1"), (13, "ag_far1"), (14, "norm1"), (15, "mixer"), (17, "branch1"),
    (18, "merge1"), (20, "finish1"),
    (22, "ag_pass2"), (23, "ag_mid2"), (24, "ag_far2"), (25, "norm2"), (26, "hidden2a"), (27, "hidden2b"),
)
MIXED = (3, 3, 2, 2, 0)
LAST = ("hidden2c", "branch2", "merge2", "finish2")


def own_part(rows, share, unit=16):
    return int(rows * share) // unit * unit


def layer(sizes, *refs):
    n_fs, n_tp, paired, splits = sizes
    (tokens, gain_first, gate_first, up_first, down_first, gain_mixer, outer_gate, inner_gate, conv_input, conv_taps,
     mixer_out, gain_last, gate_last, up_last, down_last, out,
     g1, u1, d1, mx, g2, u2, d2, raw, normed, pre, hidden, mixed, res, acc, pair_out, pair_in, side_out, side_in,
     local_sem, z_send, z_recv, y_send, y_recv, x_send, x_recv) = refs
    rows, cols = tokens.shape
    half_rows = rows // 2
    half = n_fs // 2
    f = lax.axis_index("fs")
    t = lax.axis_index("tp")
    g = lax.axis_index("grp")
    n_x = n_tp // 2
    x, core = t // 2, t % 2
    par = g % 2
    depth = mx.shape[1] // 4
    per = cols // depth

    up_fs, dn_fs = lax.rem(f + 1, n_fs), lax.rem(f + n_fs - 1, n_fs)
    ahead = lax.rem(x + 1, n_x) * 2 + core
    behind = lax.rem(x + n_x - 1, n_x) * 2 + core
    across = lax.rem(x + 2, n_x) * 2 + core
    partner = x * 2 + (1 - core)
    mate = g + 1 - 2 * par

    bufs = {"g1": g1, "u1": u1, "d1": d1, "mx": mx, "g2": g2, "u2": u2, "d2": d2}
    names = tuple(bufs)
    sources = {
        "g1": (gate_first,), "u1": (up_first,), "d1": (down_first,),
        "mx": (outer_gate, inner_gate, conv_input, mixer_out),
        "g2": (gate_last,), "u2": (up_last,), "d2": (down_last,),
    }

    loads = {}
    spare = 0
    own_tokens = pltpu.make_async_copy(tokens, raw.at[0, t], local_sem.at[spare])
    own_tokens.start()
    for name in names:
        loads[name] = []
        many = len(sources[name])
        for piece, source in enumerate(sources[name]):
            spare += 1
            place = bufs[name].at[f] if many == 1 else bufs[name].at[f, pl.ds(piece * depth, depth)]
            copy = pltpu.make_async_copy(source, place, local_sem.at[spare])
            copy.start()
            loads[name].append(copy)

    barrier = pltpu.get_barrier_semaphore()
    peers = [{"fs": up_fs}, {"fs": dn_fs}, {"tp": ahead}, {"tp": behind}, {"tp": partner}]
    if paired:
        peers.append({"grp": mate})
    for peer in peers:
        pl.semaphore_signal(barrier, inc=1, device_id=peer, device_id_type=MESH)
    pl.semaphore_wait(barrier, len(peers))

    def remote(source, target, send, recv, peer):
        return pltpu.make_async_remote_copy(
            src_ref=source, dst_ref=target, send_sem=send, recv_sem=recv, device_id=peer, device_id_type=MESH
        )

    in_flight = {}

    def send_slot(kind, count):
        queue = in_flight.setdefault(kind, [])
        if len(queue) == count:
            queue.pop(0).wait_send()
        position = in_flight.get((kind, "next"), 0)
        in_flight[(kind, "next")] = (position + 1) % count
        return position

    def ring_rows(name, direction, hop):
        alone, both = splits[name]
        start, length = par * alone, alone + both
        if hop == half:
            first = (length // 2 + 15) // 16 * 16
            start, length = (start, first) if direction == 0 else (start + first, length - first)
        return pl.ds(pl.multiple_of(start, 16), length)

    def ring_copy(name, direction, hop, send=None):
        block = lax.rem(f + n_fs - (hop - 1), n_fs) if direction == 0 else lax.rem(f + hop - 1, n_fs)
        place = bufs[name].at[block, ring_rows(name, direction, hop)]
        send = 0 if send is None else send
        return remote(
            place, place, z_send.at[direction, send], z_recv.at[names.index(name), direction, hop - 1],
            {"fs": up_fs if direction == 0 else dn_fs},
        )

    def ring_start(name, direction, hop):
        slot = send_slot(("z", direction), z_send.shape[1])
        copy = ring_copy(name, direction, hop, slot)
        copy.start()
        in_flight[("z", direction)].append(copy)

    def hand_over(name, block, hop):
        alone, both = splits[name]
        place = bufs[name].at[block, pl.ds(pl.multiple_of(par * (alone + both), 16), alone)]
        slot = send_slot("y", y_send.shape[0])
        copy = remote(place, place, y_send.at[slot], y_recv.at[names.index(name), (hop - 1) // 2], {"grp": mate})
        copy.start()
        in_flight["y"].append(copy)

    def ring_event(name, hop):
        if hop == 0:
            for copy in loads[name]:
                copy.wait()
            for direction in (0, 1):
                ring_start(name, direction, 1)
            return
        for direction in (0, 1):
            ring_copy(name, direction, hop).wait_recv()
            if hop < half:
                ring_start(name, direction, hop + 1)
        if paired:
            hand_over(name, lax.rem(f + n_fs - hop, n_fs), hop)
            if hop < half:
                hand_over(name, lax.rem(f + hop, n_fs), hop)

    def whole(name, first=1, last=half):
        if paired:
            for stop in range(first + 1, last + 1, 2):
                view = bufs[name].at[pl.ds(0, 4 if stop < half else 3), pl.ds(0, splits[name][0])]
                pltpu.make_async_copy(view, view, y_recv.at[names.index(name), stop // 2 - 1]).wait()

    x_flight = {}

    def x_start(number, phase, source, target, peer):
        if number in x_flight:
            x_flight[number].wait_send()
        copy = remote(source, target, x_send.at[number], x_recv.at[phase % 2, number], peer)
        copy.start()
        x_flight[number] = copy

    def x_wait(number, phase, place):
        remote(place, place, x_send.at[number], x_recv.at[phase % 2, number], {"tp": ahead}).wait_recv()

    low, high = pl.ds(0, half_rows), pl.ds(half_rows, half_rows)

    def ag_start(phase):
        if phase == 0:
            own_tokens.wait()
        own, own_low, own_high = raw.at[phase, t], raw.at[phase, t, low], raw.at[phase, t, high]
        x_start(0, phase, own_low, own_low, {"tp": ahead})
        x_start(1, phase, own_high, own_high, {"tp": behind})
        x_start(2, phase, own_high, own_high, {"tp": ahead})
        x_start(3, phase, own_low, own_low, {"tp": behind})
        x_start(6, phase, own, own, {"tp": partner})

    def ag_pass(phase):
        prev, nxt = raw.at[phase, behind, low], raw.at[phase, ahead, high]
        x_wait(0, phase, prev)
        x_start(4, phase, prev, prev, {"tp": ahead})
        x_wait(1, phase, nxt)
        x_start(5, phase, nxt, nxt, {"tp": behind})

    def ag_mid(phase):
        prev, nxt = raw.at[phase, behind], raw.at[phase, ahead]
        x_wait(2, phase, raw.at[phase, behind, high])
        x_start(7, phase, prev, prev, {"tp": partner})
        x_wait(3, phase, raw.at[phase, ahead, low])
        x_start(8, phase, nxt, nxt, {"tp": partner})

    def ag_far(phase):
        x_wait(4, phase, raw.at[phase, across, low])
        x_wait(5, phase, raw.at[phase, across, high])
        far = raw.at[phase, across]
        x_start(9, phase, far, far, {"tp": partner})

    def norm(phase, gain):
        for number in (6, 7, 8, 9):
            x_wait(number, phase, raw.at[phase, partner])
        step = 32

        def some(i, _):
            at = pl.ds(pl.multiple_of(i * step, step), step)
            parts = [raw[phase, j, at, :].astype(F32) for j in range(n_tp)]
            total = parts[0] * parts[0]
            for part in parts[1:]:
                total = total + part * part
            inverse = lax.rsqrt(jnp.sum(total, axis=1, keepdims=True) / (n_tp * cols) + EPS)
            for j, part in enumerate(parts):
                value = (part * inverse * gain[:, pl.ds(j * cols, cols)]).astype(BF16)
                for p in range(per):
                    normed[j * per + p, at, :] = value[:, p * depth:(p + 1) * depth]
            return 0

        lax.fori_loop(0, rows // step, some, 0)

    def hidden_part(gate, up, nearest, farthest):
        width = 128
        shifts = []
        for hop in range(nearest, farthest + 1):
            shifts += [0] if hop == 0 else [half] if hop == half else [hop, n_fs - hop]
        blocks = [lax.rem(f + shift, n_fs) for shift in shifts]

        def tile(i, _):
            span = pl.ds(pl.multiple_of(i * width, width), width)
            left = jnp.concatenate([normed[b] for b in blocks], axis=1)
            right = jnp.concatenate(
                [jnp.concatenate([gate[b, :, span], up[b, :, span]], axis=1) for b in blocks], axis=0
            )
            product = jnp.dot(left, right, preferred_element_type=F32)
            if nearest:
                product = product + pre[i]
            if farthest < half:
                pre[i] = product
            else:
                gate_pre, up_pre = product[:, :width], product[:, width:]
                hidden[:, span] = (gate_pre / (1.0 + jnp.exp(-gate_pre)) * up_pre).astype(BF16)
            return 0

        lax.fori_loop(0, gate.shape[2] // width, tile, 0)

    def hidden_stage(gate, up, nearest, farthest):
        for name in (gate, up):
            whole(name, max(nearest, 1), farthest)
        hidden_part(bufs[gate], bufs[up], nearest, farthest)

    def mixer():
        whole("mx")
        k = n_fs * depth
        left = jnp.concatenate([normed[b] for b in range(n_fs)], axis=1)
        weight = lambda p: mx[:, p * depth:(p + 1) * depth, :].reshape(k, mx.shape[2])
        width = mx.shape[2]
        pair = jnp.dot(left, jnp.concatenate([weight(1), weight(2)], axis=1), preferred_element_type=F32)
        gated = pair[:, :width] * pair[:, width:]
        place = lax.rem(lax.broadcasted_iota(jnp.int32, gated.shape, 0), SEQ_LEN)
        kernel = conv_taps.shape[0]
        convolved = gated * conv_taps[kernel - 1:kernel, :]
        for back in range(1, kernel):
            earlier = jnp.where(place >= back, pltpu.roll(gated, back, 0), 0.0)
            convolved = convolved + earlier * conv_taps[kernel - 1 - back:kernel - back, :]
        outer = jnp.dot(left, weight(0), preferred_element_type=F32)
        mixed[...] = (outer * convolved).astype(BF16)

    def block_of(left, down, lead, owner):
        tiles = [down[owner * per + p][lead:, :] if lead else down[owner * per + p] for p in range(per)]
        return jnp.dot(left[...], jnp.concatenate(tiles, axis=1), preferred_element_type=F32)

    def branch(phase, left, name, lead, factor):
        if phase != 1:
            whole(name)
        down = bufs[name]
        for number in range(10, 20):
            if number in x_flight:
                x_flight.pop(number).wait_send()

        def block(j, side):
            return block_of(left, down, lead, lax.rem(x + j, n_x) * 2 + side)

        def pair_start(j):
            x_start(10 + j, phase, pair_out.at[j], pair_in.at[phase, j], {"tp": partner})

        def pair_sum(j, keep):
            return acc[j, keep, :] + pair_in[phase, j, keep, :].astype(F32)

        def theirs(j):
            pair_out[j] = block(j, 1 - core).astype(BF16)

        theirs(2)
        theirs(1)
        pair_start(2)
        acc[2] = block(2, core)
        pair_start(1)
        theirs(3)
        x_wait(12, phase, pair_in.at[phase, 2])
        for direction, keep in ((0, low), (1, high)):
            side_out[direction, 0] = pair_sum(2, keep).astype(BF16)
        acc[1] = block(1, core)
        pair_start(3)
        for direction in (0, 1):
            side_start(phase, direction, 0)
        theirs(0)
        acc[3] = block(3, core)
        pair_start(0)
        x_wait(11, phase, pair_in.at[phase, 1])
        x_wait(13, phase, pair_in.at[phase, 3])
        for direction, near, keep in ((0, 1, high), (1, 3, low)):
            side_out[direction, 1] = pair_sum(near, keep).astype(BF16)
        acc[0] = block(0, core)
        for direction in (0, 1):
            side_start(phase, direction, 1)
        for near, keep in ((1, low), (3, high)):
            acc[near, keep, :] = pair_sum(near, keep)
        x_wait(10, phase, pair_in.at[phase, 0])
        res[...] = res[...] + factor * (acc[0] + pair_in[phase, 0].astype(F32))

    def side_start(phase, direction, order):
        x_start(
            14 + 2 * order + direction, phase, side_out.at[direction, order], side_in.at[phase, direction, order],
            {"tp": ahead if direction == 0 else behind},
        )

    def side_wait(phase, direction, order):
        x_wait(14 + 2 * order + direction, phase, side_in.at[phase, direction, order])

    def merge(phase):
        for direction, near, keep in ((0, 1, low), (1, 3, high)):
            side_wait(phase, direction, 0)
            side_out[direction, 2] = (acc[near, keep, :] + side_in[phase, direction, 0].astype(F32)).astype(BF16)
        for direction in (0, 1):
            side_start(phase, direction, 2)

    def finish(phase, factor):
        for order in (1, 2):
            for direction in (0, 1):
                side_wait(phase, direction, order)
        lo = side_in[phase, 0, 2].astype(F32) + side_in[phase, 1, 1].astype(F32)
        hi = side_in[phase, 0, 1].astype(F32) + side_in[phase, 1, 2].astype(F32)
        target = out if phase == 2 else raw.at[phase + 1, t]
        for keep, extra in ((low, lo), (high, hi)):
            target[keep, :] = (res[keep, :] + factor * extra).astype(BF16)
        if phase < 2:
            for keep, extra in ((low, lo), (high, hi)):
                res[keep, :] = res[keep, :] + factor * extra
            ag_start(phase + 1)

    def norm0():
        norm(0, gain_first)
        res[...] = raw[0, t].astype(F32)

    stages = {
        "ag_start0": lambda: ag_start(0), "ag_pass0": lambda: ag_pass(0), "ag_mid0": lambda: ag_mid(0),
        "ag_far0": lambda: ag_far(0), "norm0": norm0,
        "hidden1a": lambda: hidden_stage("g1", "u1", 0, 2), "hidden1b": lambda: hidden_stage("g1", "u1", 3, 4),
        "hidden1c": lambda: hidden_stage("g1", "u1", 5, 6), "hidden1d": lambda: hidden_stage("g1", "u1", 7, half),
        "branch0": lambda: branch(0, hidden, "d1", 0, 0.5), "merge0": lambda: merge(0),
        "finish0": lambda: finish(0, 0.5),
        "ag_pass1": lambda: ag_pass(1), "ag_mid1": lambda: ag_mid(1),
        "ag_far1": lambda: ag_far(1),
        "norm1": lambda: norm(1, gain_mixer), "mixer": mixer,
        "branch1": lambda: branch(1, mixed, "mx", 3 * depth, 1.0), "merge1": lambda: merge(1),
        "finish1": lambda: finish(1, 1.0),
        "ag_pass2": lambda: ag_pass(2), "ag_mid2": lambda: ag_mid(2),
        "ag_far2": lambda: ag_far(2),
        "norm2": lambda: norm(2, gain_last), "hidden2a": lambda: hidden_stage("g2", "u2", 0, 4),
        "hidden2b": lambda: hidden_stage("g2", "u2", 5, 6), "hidden2c": lambda: hidden_stage("g2", "u2", 7, half),
        "branch2": lambda: branch(2, hidden, "d2", 0, 0.5), "merge2": lambda: merge(2),
        "finish2": lambda: finish(2, 0.5),
    }

    plan = plan_for(half)
    for event in ring_order(half):
        with jax.named_scope("ring_%s_%d" % event):
            ring_event(*event)
        for stage in plan.get(event, ()):
            with jax.named_scope(stage):
                stages[stage]()

    for copy in list(x_flight.values()):
        copy.wait_send()
    for key, queue in in_flight.items():
        if isinstance(queue, list):
            for copy in queue:
                copy.wait_send()


def ring_order(half):
    events = []
    lead = half // 2
    for hop in range(half + 1):
        events += [(name, hop) for name in ("d1", "g1", "u1")]
        if lead <= hop < half:
            events.append(("mx", hop - lead))
        if hop == half - 1:
            events += [(name, 0) for name in ("d2", "g2", "u2")]
    late = [(name, hop) for hop in range(1, half + 1) for name in ("d2", "g2", "u2")]
    for hop in range(half - lead, half + 1):
        events.append(("mx", hop))
        for _ in range(MIXED[hop - half + lead] if half == 8 else 2):
            events.append(late.pop(0))
    return events + late


def plan_for(half):
    events = ring_order(half)
    plan = {}
    if half != 8:
        every = [stage for _, _, stages in EARLY for stage in stages] + [stage for _, stage in LATE]
        plan[events[-1]] = tuple(every) + LAST
        return plan
    for anchor, offset, stages in EARLY:
        plan.setdefault(events[events.index(anchor) + offset], []).extend(stages)
    base = events.index(("u1", half))
    for offset, stage in LATE:
        plan.setdefault(events[base + offset], []).append(stage)
    plan.setdefault(events[-1], []).extend(LAST)
    return plan


def fused_layer(n_fs, n_tp, n_grp, *args):
    tokens, gate, down, outer = args[0], args[2], args[4], args[6]
    rows, cols = tokens.shape
    paired = n_grp % 2 == 0
    n_x = n_tp // 2
    depth, hid = gate.shape
    chan = outer.shape[1]

    def split(length, share):
        alone = own_part(length, share) if paired else 0
        return alone, length - 2 * alone

    splits = {
        "g1": split(depth, 0.38), "u1": split(depth, 0.3), "d1": split(hid, 0.35), "mx": split(4 * depth, 0.38),
        "g2": split(depth, 0.3), "u2": split(depth, 0.3), "d2": split(hid, 0.38),
    }
    half = n_fs // 2
    wide = pltpu.VMEM((n_fs, depth, hid), BF16)
    tall = pltpu.VMEM((n_fs, hid, depth), BF16)
    gains = {1, 5, 11}
    args = [a.reshape(1, -1) if i in gains else a for i, a in enumerate(args)]
    vmem, anywhere = pl.BlockSpec(memory_space=pltpu.VMEM), pl.BlockSpec(memory_space=pl.ANY)
    in_vmem = gains | {9}
    return pl.pallas_call(
        functools.partial(layer, (n_fs, n_tp, paired, splits)),
        out_shape=jax.ShapeDtypeStruct((rows, cols), BF16),
        in_specs=[vmem if i in in_vmem else anywhere for i in range(len(args))],
        out_specs=vmem,
        scratch_shapes=[
            wide, wide, tall, pltpu.VMEM((n_fs, 4 * depth, chan), BF16), wide, wide, tall,
            pltpu.VMEM((3, n_tp, rows, cols), BF16),
            pltpu.VMEM((n_fs, rows, depth), BF16),
            pltpu.VMEM((hid // 128, rows, 256), F32),
            pltpu.VMEM((rows, hid), BF16),
            pltpu.VMEM((rows, chan), BF16),
            pltpu.VMEM((rows, cols), F32),
            pltpu.VMEM((n_x, rows, cols), F32),
            pltpu.VMEM((n_x, rows, cols), BF16),
            pltpu.VMEM((3, n_x, rows, cols), BF16),
            pltpu.VMEM((2, 3, rows // 2, cols), BF16),
            pltpu.VMEM((3, 2, 3, rows // 2, cols), BF16),
            pltpu.SemaphoreType.DMA((11,)),
            pltpu.SemaphoreType.DMA((2, 4)),
            pltpu.SemaphoreType.DMA((7, 2, half)),
            pltpu.SemaphoreType.DMA((4,)),
            pltpu.SemaphoreType.DMA((7, half // 2)),
            pltpu.SemaphoreType.DMA((20,)),
            pltpu.SemaphoreType.DMA((2, 20)),
        ],
        compiler_params=pltpu.CompilerParams(
            collective_id=0, has_side_effects=True, vmem_limit_bytes=60 * 1024 * 1024
        ),
        name="fused_layer",
    )(*args)


def solution(mesh):
    in_specs = (
        P(("grp", "fs"), "tp"),
        P(),
        P("fs", "tp"),
        P("fs", "tp"),
        P("tp", "fs"),
        P(),
        P("fs", "tp"),
        P("fs", "tp"),
        P("fs", "tp"),
        P(None, "tp"),
        P("tp", "fs"),
        P(),
        P("fs", "tp"),
        P("fs", "tp"),
        P("tp", "fs"),
    )
    out_specs = P(("grp", "fs"), "tp")
    body = functools.partial(fused_layer, mesh.shape["fs"], mesh.shape["tp"], mesh.shape["grp"])
    return jax.shard_map(body, mesh=mesh, in_specs=in_specs, out_specs=out_specs, check_vma=False)
```

time: 184 us -> 175 us (0.951)
  Pallas kernels: 182 us -> 174 us
    pallas_call x1, Pallas kernels: 182 us -> 174 us  [fused_layer(): pl.pallas_call(functools.partial(layer, (n_fs, n_tp, paired, splits)), ou...]
where the time goes in v2:
time: 175 us
  Pallas kernels  174 us (99%)
    pallas_call x1, Pallas kernels, fused_layer(): pl.pallas_call(functools.partial(layer, (n_fs, n_tp, paired, splits)), ou...  174 us

profile of v2, /device:TPU:33, one launch (start us, length us, event | category | flops | bytes accessed | tf_op | source)
XLA Modules:
  0.0 175.3 jit_solution(411457946056831901)
XLA Ops:
  0.0 173.7 %fused_layer.1 = bf16[384,256]{1,0:T(8,128)(2,1)} custom-call(bf16[384,256]{1,0:T(8,128)(2,1)} %refs_0_.1, f32[1,2048]{1,0:T(1,128)} %bitcast.3, bf16[128,640]{1,0:T(8,128)(2,1)} %refs_2_.1, bf16[128,640]{1,0:T(8,128)(2,1)} %refs_3_.1, bf16[640,128]{1,0:T(8,128)(2,1)} %refs_4_.1, f32[1,2048]{1,0:T(1,128)} %bitcast.4, bf16[128,128]{1,0:T(8,128)(2,1)} %refs_6_.1, ...), custom_call_target="tpu_custom_call" | custom-call | tf_op jit(solution)/shard_map/fused_layer/pallas_call | solution.py:450
  173.7 1.6 copy.17

commit v3 on v2

--- a/solution.py
+++ b/solution.py
@@ -22,12 +22,9 @@
     (("u1", 6), 1, ("hidden1c",)),
 )
 LATE = (
-    (2, "hidden1d"), (3, "branch0"), (6, "merge0"), (8, "finish0"),
-    (10, "ag_pass1"), (11, "ag_mid1"), (13, "ag_far1"), (14, "norm1"), (15, "mixer"), (17, "branch1"),
-    (18, "merge1"), (20, "finish1"),
-    (22, "ag_pass2"), (23, "ag_mid2"), (24, "ag_far2"), (25, "norm2"), (26, "hidden2a"), (27, "hidden2b"),
+    (2, "hidden1d"), (3, "branch0"), (6, "merge0"), (8, "finish0"), (10, "ag_pass1"), (11, "ag_mid1"), (13, "ag_far1"), (14, "norm1"), (15, "mixer"), (16, "branch1"), (17, "merge1"), (19, "finish1"), (21, "ag_pass2"), (22, "ag_mid2"), (23, "ag_far2"), (24, "norm2"), (25, "hidden2a"), (26, "hidden2b"),
 )
-MIXED = (3, 3, 2, 2, 0)
+MIXED = (3, 3, 3, 0)
 LAST = ("hidden2c", "branch2", "merge2", "finish2")
 
 
@@ -393,14 +390,14 @@
 
 def ring_order(half):
     events = []
-    lead = half // 2
+    lead = half // 2 - 1
     for hop in range(half + 1):
         events += [(name, hop) for name in ("d1", "g1", "u1")]
         if lead <= hop < half:
             events.append(("mx", hop - lead))
         if hop == half - 1:
-            events += [(name, 0) for name in ("d2", "g2", "u2")]
-    late = [(name, hop) for hop in range(1, half + 1) for name in ("d2", "g2", "u2")]
+            events += [(name, 0) for name in ("g2", "u2", "d2")]
+    late = [(name, hop) for hop in range(1, half + 1) for name in ("g2", "u2", "d2")]
     for hop in range(half - lead, half + 1):
         events.append(("mx", hop))
         for _ in range(MIXED[hop - half + lead] if half == 8 else 2):

time: 175 us -> 172 us (0.983)
  Pallas kernels: 174 us -> 170 us
    pallas_call x1, Pallas kernels: 174 us -> 170 us  [fused_layer(): pl.pallas_call(functools.partial(layer, (n_fs, n_tp, paired, splits)), ou...]
where the time goes in v3:
time: 172 us
  Pallas kernels  170 us (99%)
    pallas_call x1, Pallas kernels, fused_layer(): pl.pallas_call(functools.partial(layer, (n_fs, n_tp, paired, splits)), ou...  170 us

profile of v3, /device:TPU:33, one launch (start us, length us, event | category | flops | bytes accessed | tf_op | source)
XLA Modules:
  0.0 172.1 jit_solution(14184563214830714384)
XLA Ops:
  0.0 170.5 %fused_layer.1 = bf16[384,256]{1,0:T(8,128)(2,1)} custom-call(bf16[384,256]{1,0:T(8,128)(2,1)} %refs_0_.1, f32[1,2048]{1,0:T(1,128)} %bitcast.3, bf16[128,640]{1,0:T(8,128)(2,1)} %refs_2_.1, bf16[128,640]{1,0:T(8,128)(2,1)} %refs_3_.1, bf16[640,128]{1,0:T(8,128)(2,1)} %refs_4_.1, f32[1,2048]{1,0:T(1,128)} %bitcast.4, bf16[128,128]{1,0:T(8,128)(2,1)} %refs_6_.1, ...), custom_call_target="tpu_custom_call" | custom-call | tf_op jit(solution)/shard_map/fused_layer/pallas_call | solution.py:447
  170.5 1.6 copy.17

commit v4 on v3

--- a/solution.py
+++ b/solution.py
@@ -22,7 +22,7 @@
     (("u1", 6), 1, ("hidden1c",)),
 )
 LATE = (
-    (2, "hidden1d"), (3, "branch0"), (6, "merge0"), (8, "finish0"), (10, "ag_pass1"), (11, "ag_mid1"), (13, "ag_far1"), (14, "norm1"), (15, "mixer"), (16, "branch1"), (17, "merge1"), (19, "finish1"), (21, "ag_pass2"), (22, "ag_mid2"), (23, "ag_far2"), (24, "norm2"), (25, "hidden2a"), (26, "hidden2b"),
+    (2, "hidden1d"), (3, "branch0"), (6, "merge0"), (8, "finish0"), (10, "ag_pass1"), (11, "ag_mid1"), (13, "ag_far1"), (14, "norm1"), (15, "mixer"), (16, "branch1"), (17, "merge1"), (19, "finish1"), (22, "ag_pass2"), (22, "ag_mid2"), (23, "ag_far2"), (24, "norm2"), (25, "hidden2a"),
 )
 MIXED = (3, 3, 3, 0)
 LAST = ("hidden2c", "branch2", "merge2", "finish2")
@@ -366,8 +366,8 @@
         "finish1": lambda: finish(1, 1.0),
         "ag_pass2": lambda: ag_pass(2), "ag_mid2": lambda: ag_mid(2),
         "ag_far2": lambda: ag_far(2),
-        "norm2": lambda: norm(2, gain_last), "hidden2a": lambda: hidden_stage("g2", "u2", 0, 4),
-        "hidden2b": lambda: hidden_stage("g2", "u2", 5, 6), "hidden2c": lambda: hidden_stage("g2", "u2", 7, half),
+        "norm2": lambda: norm(2, gain_last), "hidden2a": lambda: hidden_stage("g2", "u2", 0, 6),
+        "hidden2c": lambda: hidden_stage("g2", "u2", 7, half),
         "branch2": lambda: branch(2, hidden, "d2", 0, 0.5), "merge2": lambda: merge(2),
         "finish2": lambda: finish(2, 0.5),
     }

time: 172 us -> 172 us (level)
  no operation moved by 1% of the time
where the time goes in v4:
time: 172 us
  Pallas kernels  171 us (99%)
    pallas_call x1, Pallas kernels, fused_layer(): pl.pallas_call(functools.partial(layer, (n_fs, n_tp, paired, splits)), ou...  171 us

profile of v4, /device:TPU:33, one launch (start us, length us, event | category | flops | bytes accessed | tf_op | source)
XLA Modules:
  0.0 172.2 jit_solution(14418442569839695493)
XLA Ops:
  0.0 170.5 %fused_layer.1 = bf16[384,256]{1,0:T(8,128)(2,1)} custom-call(bf16[384,256]{1,0:T(8,128)(2,1)} %refs_0_.1, f32[1,2048]{1,0:T(1,128)} %bitcast.3, bf16[128,640]{1,0:T(8,128)(2,1)} %refs_2_.1, bf16[128,640]{1,0:T(8,128)(2,1)} %refs_3_.1, bf16[640,128]{1,0:T(8,128)(2,1)} %refs_4_.1, f32[1,2048]{1,0:T(1,128)} %bitcast.4, bf16[128,128]{1,0:T(8,128)(2,1)} %refs_6_.1, ...), custom_call_target="tpu_custom_call" | custom-call | tf_op jit(solution)/shard_map/fused_layer/pallas_call | solution.py:447
  170.5 1.6 copy.17
